TPU v7x, 32 devices: a whole 2x2x4 slice. The times are simulated.
32 devices in a mesh: kv: 8 (over z, x), tp: 4 (over y, core).
Axes of the slice: x: 2, y: 2, z: 4, core: 2. Of those that a mesh axis runs over, the one named last changes fastest.
Arguments:
- hidden: bfloat16 [128, 4, 2048], P(None, None, 'kv'), may hold values from -18 to 18
- norm_gain: float32 [2048], replicated, may hold values from 0.1 to 1.9
- w_query: bfloat16 [2048, 1024], P(None, 'tp'), may hold values from -0.125 to 0.125
- w_forget: bfloat16 [2048, 1024], P(None, 'tp'), may hold values from -0.125 to 0.125
- w_input: bfloat16 [2048, 1024], P(None, 'tp'), may hold values from -0.125 to 0.125
- w_outgate: bfloat16 [2048, 1024], P(None, 'tp'), may hold values from -0.125 to 0.125
- w_out: bfloat16 [1024, 2048], replicated, may hold values from -0.1875 to 0.1875
- floor: float32 [1024], P('tp'), may hold values from 0 to 0.95
- head_gain: float32 [128], replicated, may hold values from 0.1 to 1.9
- base_state: float32 [128, 8, 128, 128], P('kv', 'tp'), may hold values from -4 to 4
- prev_forget: bfloat16 [128, 4, 1024], P('kv', None, 'tp'), may hold values from -6 to 6
- prev_input: bfloat16 [128, 4, 1024], P('kv', None, 'tp'), may hold values from -6 to 6
- accepted: int32 [128], P('kv'), may hold values from 0 to 4
Outputs:
- mixed: bfloat16 [128, 4, 2048], P(None, None, 'kv')
- taken_state: float32 [128, 8, 128, 128], P('kv', 'tp')
All inputs are finite; a program needn't handle non-finite values.
Results may differ from a plain program's by a relative error of at most 0.014.
Values may be sent and summed in bfloat16 or wider, within the bound.
A program may use at most 64 MiB of HBM per device.

v0:
```python
import jax
import jax.numpy as jnp
from jax import lax
from jax.sharding import PartitionSpec as P

D = 2048
HEAD_DIM = 128
PROPS = 4


def shards(
    hidden,
    norm_gain,
    w_query,
    w_forget,
    w_input,
    w_outgate,
    w_out,
    floor,
    head_gain,
    base_state,
    prev_forget,
    prev_input,
    accepted,
):
    arrived = lax.all_to_all(hidden, "kv", split_axis=0, concat_axis=2, tiled=True)
    whole_vals = arrived.astype(jnp.float32)
    row_sums = jnp.sum(whole_vals * whole_vals, axis=2)
    normed = (whole_vals * lax.rsqrt(row_sums / D + 1e-06)[..., None] * norm_gain).astype(
        jnp.bfloat16
    )
    query_pre = jnp.dot(normed, w_query, preferred_element_type=jnp.float32).astype(jnp.bfloat16)
    forget_pre = jnp.dot(normed, w_forget, preferred_element_type=jnp.float32).astype(jnp.bfloat16)
    input_pre = jnp.dot(normed, w_input, preferred_element_type=jnp.float32).astype(jnp.bfloat16)
    gate_pre = jnp.dot(normed, w_outgate, preferred_element_type=jnp.float32).astype(jnp.bfloat16)
    seq_local = normed.shape[0]
    head_local = w_query.shape[1] // HEAD_DIM
    shape = (seq_local, PROPS, head_local, HEAD_DIM)
    query = jax.nn.silu(query_pre.astype(jnp.float32)).reshape(shape)
    forget = (floor + (1.0 - floor) * jax.nn.sigmoid(forget_pre.astype(jnp.float32))).reshape(shape)
    value = input_pre.astype(jnp.float32).reshape(shape)
    prev_f = (floor + (1.0 - floor) * jax.nn.sigmoid(prev_forget.astype(jnp.float32))).reshape(
        shape
    )
    prev_v = prev_input.astype(jnp.float32).reshape(shape)
    state = base_state
    for step in range(PROPS):
        live = (step < accepted)[:, None, None, None]
        moved = (
            prev_f[:, step][..., None] * state
            + (1.0 - prev_f[:, step])[..., None] * prev_v[:, step][:, :, None, :]
        )
        state = jnp.where(live, moved, state)
    taken_state = state
    outputs = []
    for step in range(PROPS):
        state = (
            forget[:, step][..., None] * state
            + (1.0 - forget[:, step])[..., None] * value[:, step][:, :, None, :]
        )
        outputs.append(
            jnp.einsum("bhk,bhkv->bhv", query[:, step], state, precision=lax.Precision.HIGHEST)
        )
    result = jnp.stack(outputs, axis=1)
    scaled = (
        result * lax.rsqrt(jnp.mean(result * result, axis=-1, keepdims=True) + 1e-05) * head_gain
    )
    gated = scaled * jax.nn.silu(gate_pre.astype(jnp.float32)).reshape(shape)
    mixed_heads = gated.reshape(seq_local, PROPS, head_local * HEAD_DIM).astype(jnp.bfloat16)
    own_rows = mixed_heads.shape[2]
    w_rows = lax.dynamic_slice_in_dim(w_out, lax.axis_index("tp") * own_rows, own_rows, 0)
    partial_value = jnp.dot(mixed_heads, w_rows, preferred_element_type=jnp.float32)
    finished = lax.psum(partial_value, "tp").astype(jnp.bfloat16)
    mixed = lax.all_to_all(finished, "kv", split_axis=2, concat_axis=0, tiled=True)
    return (mixed, taken_state)


def solution(mesh):
    placed = (
        P(None, None, "kv"),
        P(),
        P(None, "tp"),
        P(None, "tp"),
        P(None, "tp"),
        P(None, "tp"),
        P(),
        P("tp"),
        P(),
        P("kv", "tp", None, None),
        P("kv", None, "tp"),
        P("kv", None, "tp"),
        P("kv"),
    )
    return jax.shard_map(
        shards,
        mesh=mesh,
        in_specs=placed,
        out_specs=(P(None, None, "kv"), P("kv", "tp", None, None)),
        check_vma=False,
    )
```

profile of v0, /device:TPU:0, one launch (start us, length us, event | category | flops | bytes accessed | tf_op | source)
XLA Modules:
  0.0 96.0 jit_solution(18002514994027775703)
XLA Ops:
  0.6 0.0 copy-start
  0.6 7.4 %all-to-all-start = ((bf16[128,4,256]{2,1,0:T(4,128)(2,1)}), bf16[128,4,256]{2,1,0:T(4,128)(2,1)S(1)}, u32[]{:S(2)}, u32[]{:S(2)}) async-start(bf16[128,4,256]{2,1,0:T(4,128)(2,1)} %param.13), calls=%async_computation | async-start | bytes 524288 | tf_op jit(solution)/shard_map/all_to_all | solution.py:26
  8.1 0.7 broadcast_subtract_fusion.8
  8.8 0.6 copy-done.3
  9.3 0.8 multiply_add_fusion.9
  10.2 1.2 %broadcast_bitcast_fusion = f32[256]{0:T(256)} fusion(f32[128]{0:T(128)} %param.21), kind=kLoop, calls=%fused_computation.82 | loop fusion | bytes 1536 | tf_op jit(solution)/shard_map/mul | solution.py:66
  11.5 1.3 %broadcast_compare_fusion.3 = (pred[16]{0:T(512)(128)(4,1)}, pred[16]{0:T(512)(128)(4,1)}, pred[16]{0:T(512)(128)(4,1)}, pred[16]{0:T(512)(128)(4,1)}) fusion(s32[16]{0:T(128)} %param.25), kind=kLoop, calls=%fused_computation.88 | loop fusion | flops 64 | bytes 128 | tf_op jit(solution)/shard_map/gt | solution.py:48
  12.7 0.8 reshape.130
  13.5 0.6 slice_bitcast_fusion.10
  14.1 7.1 %add_select_fusion = f32[16,2,128,128]{3,2,1,0:T(8,128)S(1)} fusion(f32[16,2,128,128]{3,2,1,0:T(8,128)} %param.22, f32[16,2,128]{2,1,0:T(2,128)} %get-tuple-element.29, f32[16,2,128]{2,1,0:T(2,128)S(1)} %get-tuple-element.25, f32[16,2,128]{2,1,0:T(2,128)} %get-tuple-element.27, f32[16,2,128]{2,1,0:T(2,128)S(1)} %get-tuple-element.24, ...), kind=kLoop, calls=%fused_computation.7 | loop fusion | flops 8388608 | bytes 4390976 | tf_op jit(solution)/shard_map/jit(_where)/select_n | solution.py:53
  21.3 0.0 copy-start.1
  21.3 0.0 copy-start.5
  21.3 0.0 copy-start.2
  21.3 0.0 copy-start.4
  21.3 0.0 all-to-all-done
  21.3 0.2 multiply_reduce_fusion
  21.6 0.1 copy.55
  21.7 0.1 convert_element_type.70
  21.7 1.1 %copy.38 = f32[16,4,8,256]{3,2,0,1:T(8,128)} copy(f32[16,4,8,256]{3,1,0,2:T(4,128)S(1)} %bitcast.141) | data formatting | bytes 1048576 | tf_op jit(solution)/shard_map/convert_element_type | solution.py:27
  22.8 1.9 %reshape.128 = f32[16,4,2048]{2,0,1:T(8,128)} reshape(f32[16,4,8,256]{3,2,0,1:T(8,128)} %copy.38) | data formatting | bytes 1048576 | tf_op jit(solution)/shard_map/convert_element_type | solution.py:27
  24.8 0.0 copy-done.5
  24.8 1.2 %multiply_convert_fusion = bf16[16,4,2048]{2,0,1:T(8,128)(2,1)S(1)} fusion(f32[16,4,2048]{2,0,1:T(8,128)} %reshape.128, f32[2048]{0:T(1024)S(1)} %copy-done.5, f32[16,4]{0,1:T(4,128)S(1)} %add_rsqrt_fusion.1), kind=kLoop, calls=%fused_computation.43 | loop fusion | flops 393216 | bytes 794880 | tf_op jit(solution)/shard_map/convert_element_type | solution.py:29
  25.9 0.0 copy-done.2
  25.9 0.0 copy-done.4
  25.9 1.5 %fusion.14 = f32[16,4,256]{2,0,1:T(8,128)S(1)} fusion(bf16[16,4,2048]{2,0,1:T(8,128)(2,1)S(1)} %multiply_convert_fusion, bf16[2048,256]{1,0:T(8,128)(2,1)} %param.16, f32[256]{0:T(256)S(1)} %copy-done.4, f32[256]{0:T(256)S(1)} %copy-done.2), kind=kOutput, calls=%fused_computation.21 | convolution fusion | flops 67223552 | bytes 1378304 | tf_op jit(solution)/shard_map/dot_general | solution.py:33
  27.5 1.5 %fusion.7 = f32[16,4,256]{2,0,1:T(8,128)S(1)} fusion(bf16[16,4,2048]{2,0,1:T(8,128)(2,1)S(1)} %multiply_convert_fusion, bf16[2048,256]{1,0:T(8,128)(2,1)} %param.17), kind=kOutput, calls=%fused_computation.13 | convolution fusion | flops 67141632 | bytes 1376256 | tf_op jit(solution)/shard_map/dot_general | solution.py:34
  29.1 0.7 reshape.132
  29.7 2.2 %divide_multiply_fusion = f32[16,4,256]{2,0,1:T(8,128)} fusion(bf16[16,4,2048]{2,0,1:T(8,128)(2,1)S(1)} %multiply_convert_fusion, bf16[2048,256]{1,0:T(8,128)(2,1)} %param.15), kind=kOutput, calls=%fused_computation.53 | convolution fusion | flops 67207168 | bytes 1376256 | tf_op jit(solution)/shard_map/dot_general | solution.py:32
  31.9 0.9 reshape.121
  32.8 0.8 slice_bitcast_fusion.6
  33.6 2.8 %fusion.4 = f32[16,2,1,128]{3,2,1,0:T(1,128)S(1)} fusion(f32[16,2,128,1]{2,3,1,0:T(1,128)S(1)} %bitcast.146, f32[16,2,128,128]{3,2,1,0:T(8,128)S(1)} %add_select_fusion, f32[16,2,128]{2,1,0:T(2,128)S(1)} %get-tuple-element.14, f32[16,2,128]{2,1,0:T(2,128)S(1)} %get-tuple-element.10, f32[16,2,128]{2,1,0:T(2,128)S(1)} %get-tuple-element.37), kind=kOutput, calls=%fused_computation.8 | convolution fusion | flops 7864320 | bytes 2179072 | tf_op jit(solution)/shard_map/bhk,bhkv->bhv/dot_general | solution.py:62
  36.4 4.3 %fusion.35 = f32[16,2,1,128]{3,2,1,0:T(1,128)S(1)} fusion(f32[16,2,128,1]{2,3,1,0:T(1,128)S(1)} %bitcast.155, f32[16,2,128,128]{3,2,1,0:T(8,128)S(1)} %add_select_fusion, f32[16,2,128]{2,1,0:T(2,128)S(1)} %get-tuple-element.17, f32[16,2,128]{2,1,0:T(2,128)S(1)} %get-tuple-element.13, f32[16,2,128]{2,1,0:T(2,128)S(1)} %get-tuple-element.34, ...), kind=kOutput, calls=%fused_computation.45 | convolution fusion | flops 9437184 | bytes 2228224 | tf_op jit(solution)/shard_map/bhk,bhkv->bhv/dot_general | solution.py:62
  40.7 6.1 %fusion.5 = f32[16,2,1,128]{3,2,1,0:T(1,128)S(1)} fusion(f32[16,2,128,1]{2,3,1,0:T(1,128)S(1)} %bitcast.154, f32[16,2,128]{2,1,0:T(2,128)S(1)} %get-tuple-element.16, f32[16,2,128]{2,1,0:T(2,128)S(1)} %get-tuple-element.12, f32[16,2,128]{2,1,0:T(2,128)S(1)} %get-tuple-element.35, f32[16,2,128,128]{3,2,1,0:T(8,128)S(1)} %add_select_fusion, ...), kind=kOutput, calls=%fused_computation.9 | convolution fusion | flops 11010048 | bytes 2277376 | tf_op jit(solution)/shard_map/bhk,bhkv->bhv/dot_general | solution.py:62
  46.8 0.0 copy-done.1
  46.8 0.0 copy-start.6
  46.8 7.2 %fusion = f32[16,2,1,128]{3,2,1,0:T(1,128)S(1)} fusion(f32[16,2,128,1]{2,3,1,0:T(1,128)S(1)} %bitcast.153, f32[16,2,128]{2,1,0:T(2,128)S(1)} %get-tuple-element.15, f32[16,2,128]{2,1,0:T(2,128)S(1)} %get-tuple-element.11, f32[16,2,128]{2,1,0:T(2,128)S(1)} %get-tuple-element.36, f32[16,2,128]{2,1,0:T(2,128)S(1)} %get-tuple-element.16, ...), kind=kOutput, calls=%fused_computation | convolution fusion | flops 12582912 | bytes 2326528 | tf_op jit(solution)/shard_map/bhk,bhkv->bhv/dot_general | solution.py:62
  54.1 0.1 fusion.39
  54.2 0.1 mul.343
  54.4 0.1 mul.344
  54.4 0.0 copy-done
  54.4 0.0 copy-done.6
  54.4 2.0 %fusion.16 = f32[16,4,2048]{2,0,1:T(8,128)S(1)} fusion(bf16[1024,2048]{1,0:T(8,128)(2,1)} %param.19, s32[]{:T(128)S(6)} %select_n.20, f32[16,4,256]{2,0,1:T(8,128)S(1)} %mul.344, f32[16,1,256]{2,0,1:T(8,128)S(1)} %stack.28, f32[16,1,256]{2,0,1:T(8,128)S(1)} %stack.27, f32[16,1,256]{2,0,1:T(8,128)S(1)} %stack.26, f32[16,1,256]{2,0,1:T(8,128)S(1)} %stack.25, ...), kind=kOutput, calls=%fused_computation.24 | convolution fusion | flops 134430720 | bytes 3015684 | tf_op jit(solution)/shard_map/dot_general | solution.py:72
  56.5 16.6 %all-reduce.1 = bf16[16,4,2048]{2,0,1:T(8,128)(2,1)S(1)} all-reduce(f32[16,4,2048]{2,0,1:T(8,128)S(1)} %fusion.16), channel_id=1, replica_groups=mesh['kv'=8,'tp'=4] {'tp'}, use_global_device_ids=true, to_apply=%region_3.4 | all-reduce | flops 131072 | bytes 786432 | tf_op jit(solution)/shard_map/psum | solution.py:73
  73.1 1.4 %copy.45 = bf16[16,4,2048]{0,1,2:T(4,128)(2,1)S(1)} copy(bf16[16,4,2048]{2,0,1:T(8,128)(2,1)S(1)} %all-reduce.1) | data formatting | bytes 524288 | tf_op jit(solution)/shard_map/convert_element_type | solution.py:73
  74.5 2.2 %reshape.148 = bf16[8,2,8192]{2,1,0:T(2,128)(2,1)S(1)} reshape(bf16[2048,4,16]{2,1,0:T(4,128)(2,1)S(1)} %bitcast.139) | data formatting | bytes 524288
  76.7 14.9 %all_to_all.27 = bf16[8,2,8192]{2,1,0:T(2,128)(2,1)} all-to-all(bf16[8,2,8192]{2,1,0:T(2,128)(2,1)S(1)} %reshape.148), channel_id=1, replica_groups=mesh['kv'=8,'tp'=4] {'kv'}, dimensions={0} | all-to-all | bytes 524288 | tf_op jit(solution)/shard_map/all_to_all | solution.py:74
  91.5 2.4 %reshape.149 = bf16[2048,4,16]{2,1,0:T(4,128)(2,1)S(1)} reshape(bf16[8,2,8192]{2,1,0:T(2,128)(2,1)} %all_to_all.27) | data formatting | bytes 524288
  94.0 2.0 %copy.46 = bf16[8,16,4,256]{3,2,1,0:T(4,128)(2,1)} copy(bf16[8,16,4,256]{1,2,3,0:T(4,128)(2,1)S(1)} %bitcast.140) | data formatting | bytes 524288 | tf_op jit(solution)/shard_map/all_to_all | solution.py:74
  (14 shorter events, 0.3 us)
Async XLA Ops:
  0.6 53.8 %copy-start = (bf16[2048,256]{1,0:T(8,128)(2,1)S(1)}, bf16[2048,256]{1,0:T(8,128)(2,1)}, u32[]{:S(2)}) copy-start(bf16[2048,256]{1,0:T(8,128)(2,1)} %param.18) | copy-start | bytes 3145732
  0.6 20.7 %all-to-all-start = ((bf16[128,4,256]{2,1,0:T(4,128)(2,1)}), bf16[128,4,256]{2,1,0:T(4,128)(2,1)S(1)}, u32[]{:S(2)}, u32[]{:S(2)}) async-start(bf16[128,4,256]{2,1,0:T(4,128)(2,1)} %param.13), calls=%async_computation | async-start | bytes 524288 | tf_op jit(solution)/shard_map/all_to_all | solution.py:26
  8.8 0.6 copy-start.3
  21.3 25.5 %copy-start.1 = (f32[16,2,128,128]{3,2,1,0:T(8,128)}, f32[16,2,128,128]{3,2,1,0:T(8,128)S(1)}, u32[]{:S(2)}) copy-start(f32[16,2,128,128]{3,2,1,0:T(8,128)S(1)} %add_select_fusion) | copy-start | bytes 6291460
  21.3 3.5 %copy-start.5 = (f32[2048]{0:T(1024)S(1)}, f32[2048]{0:T(1024)}, u32[]{:S(2)}) copy-start(f32[2048]{0:T(1024)} %param.14) | copy-start | bytes 24580
  21.3 4.6 %copy-start.2 = (f32[256]{0:T(256)S(1)}, f32[256]{0:T(256)}, u32[]{:S(2)}) copy-start(f32[256]{0:T(256)} %param.20) | copy-start | bytes 3076
  21.3 4.6 %copy-start.4 = (f32[256]{0:T(256)S(1)}, f32[256]{0:T(256)}, u32[]{:S(2)}) copy-start(f32[256]{0:T(256)} %copy-done.3) | copy-start | bytes 3076
  46.8 7.7 %copy-start.6 = (f32[256]{0:T(256)S(1)}, f32[256]{0:T(256)}, u32[]{:S(2)}) copy-start(f32[256]{0:T(256)} %broadcast_bitcast_fusion) | copy-start | bytes 3076
where the time goes:
time: 96.9 us; the launch traced here: 96 us
  blocking collectives  31.5 us (33%)
  matrix products  27.6 us (28%)
  local copies, waits for them, and re-layouts  17 us (18%)
  other arithmetic  11.5 us (12%)
  starting transfers between devices  7.42 us (8%)
    dot_general x4, matrix products, shards(): jnp.einsum('bhk,bhkv->bhv', query[:, step], state, precision=lax.Precisio...  20.3 us
    psum x1, blocking collectives, shards(): finished = lax.psum(partial_value, 'tp').astype(jnp.bfloat16)  16.6 us
    all_to_all x1, blocking collectives, shards(): lax.all_to_all(finished, 'kv', split_axis=2, concat_axis=0, tiled=True)  14.9 us
    all_to_all x1, starting transfers between devices, shards(): lax.all_to_all(hidden, 'kv', split_axis=0, concat_axis=2, tiled=True)  7.42 us
    select_n x1, other arithmetic, shards(): state = jnp.where(live, moved, state)  7.13 us
    unnamed x17, local copies, waits for them, and re-layouts  5.27 us
    convert_element_type x2, local copies, waits for them, and re-layouts, shards(): whole_vals = arrived.astype(jnp.float32)  3.03 us
    dot_general x1, matrix products, shards(): jnp.dot(normed, w_query, preferred_element_type=jnp.float32)  2.17 us
  transfers between devices with their start and end apart: 1, of which 0 were waited for; matrix products, arithmetic and copies ran while one was open for 13% of the time, Pallas kernels for 0%

commit v1 on v0

--- a/solution.py
+++ b/solution.py
@@ -70,7 +70,7 @@
     own_rows = mixed_heads.shape[2]
     w_rows = lax.dynamic_slice_in_dim(w_out, lax.axis_index("tp") * own_rows, own_rows, 0)
     partial_value = jnp.dot(mixed_heads, w_rows, preferred_element_type=jnp.float32)
-    finished = lax.psum(partial_value, "tp").astype(jnp.bfloat16)
+    finished = jnp.sum(lax.all_gather(partial_value, "tp"), axis=0).astype(jnp.bfloat16)
     mixed = lax.all_to_all(finished, "kv", split_axis=2, concat_axis=0, tiled=True)
     return (mixed, taken_state)
 

time: 96.9 us -> 120 us (1.24)
  waiting for transfers between devices: 0.01 us -> 24.1 us
  blocking collectives: 31.5 us -> 14.7 us
  between operations: 0.93 us -> 14.3 us
  other arithmetic: 11.5 us -> 13.3 us
    all_gather x0 -> x1, waiting for transfers between devices: none -> 24.1 us  [shards(): lax.all_gather(partial_value, 'tp')]
    psum x1 -> x0, blocking collectives: 16.6 us -> none  [shards(): finished = lax.psum(partial_value, 'tp').astype(jnp.bfloat16)]
    reduce_sum x0 -> x1, other arithmetic: none -> 1.78 us  [shards(): jnp.sum(lax.all_gather(partial_value, 'tp'), axis=0).astype(jnp.bfloat16)]
    unnamed x17 -> x18, local copies, waits for them, and re-layouts: 5.27 us -> 6.17 us
  transfers between devices with their start and end apart: 1 -> 2, of which waited for: 0 -> 1; matrix products, arithmetic and copies ran while one was open for 13% -> 11% of each run, Pallas kernels for 0% -> 0%
where the time goes in v1:
time: 120 us; the launch traced here: 119 us
  matrix products  28.4 us (24%)
  waiting for transfers between devices  24.1 us (20%)
  local copies, waits for them, and re-layouts  17 us (14%)
  blocking collectives  14.7 us (12%)
  between operations  14.3 us (12%)
  other arithmetic  13.3 us (11%)
  starting transfers between devices  7.46 us (6%)
    all_gather x1, waiting for transfers between devices, shards(): lax.all_gather(partial_value, 'tp')  24.1 us
    dot_general x4, matrix products, shards(): jnp.einsum('bhk,bhkv->bhv', query[:, step], state, precision=lax.Precisio...  20.3 us
    all_to_all x1, blocking collectives, shards(): lax.all_to_all(finished, 'kv', split_axis=2, concat_axis=0, tiled=True)  14.7 us
    all_to_all x1, starting transfers between devices, shards(): lax.all_to_all(hidden, 'kv', split_axis=0, concat_axis=2, tiled=True)  7.42 us
    select_n x1, other arithmetic, shards(): state = jnp.where(live, moved, state)  7.13 us
    unnamed x18, local copies, waits for them, and re-layouts  6.17 us
    convert_element_type x2, local copies, waits for them, and re-layouts, shards(): whole_vals = arrived.astype(jnp.float32)  3.01 us
    dot_general x1, matrix products, shards(): jnp.dot(mixed_heads, w_rows, preferred_element_type=jnp.float32)  2.85 us
  transfers between devices with their start and end apart: 2, of which 1 were waited for; matrix products, arithmetic and copies ran while one was open for 11% of the time, Pallas kernels for 0%

profile of v1, /device:TPU:0, one launch (start us, length us, event | category | flops | bytes accessed | tf_op | source)
XLA Modules:
  0.0 119.4 jit_solution(5883144368100798663)
XLA Ops:
  7.2 0.0 copy-start
  7.2 7.4 %all-to-all-start = ((bf16[128,4,256]{2,1,0:T(4,128)(2,1)}), bf16[128,4,256]{2,1,0:T(4,128)(2,1)S(1)}, u32[]{:S(2)}, u32[]{:S(2)}) async-start(bf16[128,4,256]{2,1,0:T(4,128)(2,1)} %param.13), calls=%async_computation | async-start | bytes 524288 | tf_op jit(solution)/shard_map/all_to_all | solution.py:26
  14.6 0.0 all-gather.3.cloned.1.call-start
  14.7 0.7 broadcast_subtract_fusion.8
  15.3 0.6 copy-done.3
  15.9 0.8 multiply_add_fusion.9
  16.8 1.2 %broadcast_bitcast_fusion = f32[256]{0:T(256)} fusion(f32[128]{0:T(128)} %param.21), kind=kLoop, calls=%fused_computation.82 | loop fusion | bytes 1536 | tf_op jit(solution)/shard_map/mul | solution.py:66
  18.0 1.2 %broadcast_compare_fusion.3 = (pred[16]{0:T(512)(128)(4,1)}, pred[16]{0:T(512)(128)(4,1)}, pred[16]{0:T(512)(128)(4,1)}, pred[16]{0:T(512)(128)(4,1)}) fusion(s32[16]{0:T(128)} %param.25), kind=kLoop, calls=%fused_computation.88 | loop fusion | flops 64 | bytes 128 | tf_op jit(solution)/shard_map/gt | solution.py:48
  19.3 0.8 reshape.130
  20.1 0.6 slice_bitcast_fusion.10
  20.7 7.1 %add_select_fusion = f32[16,2,128,128]{3,2,1,0:T(8,128)S(1)} fusion(f32[16,2,128,128]{3,2,1,0:T(8,128)} %param.22, f32[16,2,128]{2,1,0:T(2,128)} %get-tuple-element.39, f32[16,2,128]{2,1,0:T(2,128)S(1)} %get-tuple-element.35, f32[16,2,128]{2,1,0:T(2,128)} %get-tuple-element.37, f32[16,2,128]{2,1,0:T(2,128)S(1)} %get-tuple-element.34, ...), kind=kLoop, calls=%fused_computation.7 | loop fusion | flops 8388608 | bytes 4390976 | tf_op jit(solution)/shard_map/jit(_where)/select_n | solution.py:53
  27.8 0.0 copy-start.1
  27.8 0.0 copy-start.5
  27.9 0.0 copy-start.2
  27.9 0.0 all-to-all-done
  27.9 0.2 multiply_reduce_fusion
  28.1 0.1 copy.85
  28.2 0.1 convert_element_type.70
  28.3 1.1 copy.64
  29.4 1.9 %reshape.128 = f32[16,4,2048]{2,0,1:T(8,128)} reshape(f32[16,4,8,256]{3,2,0,1:T(8,128)} %copy.64) | data formatting | bytes 1048576 | tf_op jit(solution)/shard_map/convert_element_type | solution.py:27
  31.3 1.2 multiply_convert_fusion
  32.5 0.0 copy-done.2
  32.5 0.0 copy-done.4
  32.5 1.5 %fusion.14 = f32[16,4,256]{2,0,1:T(8,128)S(1)} fusion(bf16[16,4,2048]{2,0,1:T(8,128)(2,1)S(1)} %multiply_convert_fusion, bf16[2048,256]{1,0:T(8,128)(2,1)} %param.16, f32[256]{0:T(256)S(1)} %copy-done.4, f32[256]{0:T(256)S(1)} %copy-done.2), kind=kOutput, calls=%fused_computation.21 | convolution fusion | flops 67223552 | bytes 1378304 | tf_op jit(solution)/shard_map/dot_general | solution.py:33
  34.1 1.5 %fusion.7 = f32[16,4,256]{2,0,1:T(8,128)S(1)} fusion(bf16[16,4,2048]{2,0,1:T(8,128)(2,1)S(1)} %multiply_convert_fusion, bf16[2048,256]{1,0:T(8,128)(2,1)} %param.17), kind=kOutput, calls=%fused_computation.13 | convolution fusion | flops 67141632 | bytes 1376256 | tf_op jit(solution)/shard_map/dot_general | solution.py:34
  35.6 0.7 reshape.132
  36.3 2.2 %divide_multiply_fusion = f32[16,4,256]{2,0,1:T(8,128)} fusion(bf16[16,4,2048]{2,0,1:T(8,128)(2,1)S(1)} %multiply_convert_fusion, bf16[2048,256]{1,0:T(8,128)(2,1)} %param.15), kind=kOutput, calls=%fused_computation.53 | convolution fusion | flops 67207168 | bytes 1376256 | tf_op jit(solution)/shard_map/dot_general | solution.py:32
  38.4 0.9 reshape.121
  39.4 0.8 slice_bitcast_fusion.6
  40.1 2.8 %fusion.4 = f32[16,2,1,128]{3,2,1,0:T(1,128)S(1)} fusion(f32[16,2,128,1]{2,3,1,0:T(1,128)S(1)} %bitcast.149, f32[16,2,128,128]{3,2,1,0:T(8,128)S(1)} %add_select_fusion, f32[16,2,128]{2,1,0:T(2,128)S(1)} %get-tuple-element.24, f32[16,2,128]{2,1,0:T(2,128)S(1)} %get-tuple-element.20, f32[16,2,128]{2,1,0:T(2,128)S(1)} %get-tuple-element.47), kind=kOutput, calls=%fused_computation.8 | convolution fusion | flops 7864320 | bytes 2179072 | tf_op jit(solution)/shard_map/bhk,bhkv->bhv/dot_general | solution.py:62
  43.0 4.3 %fusion.35 = f32[16,2,1,128]{3,2,1,0:T(1,128)S(1)} fusion(f32[16,2,128,1]{2,3,1,0:T(1,128)S(1)} %bitcast.158, f32[16,2,128,128]{3,2,1,0:T(8,128)S(1)} %add_select_fusion, f32[16,2,128]{2,1,0:T(2,128)S(1)} %get-tuple-element.27, f32[16,2,128]{2,1,0:T(2,128)S(1)} %get-tuple-element.23, f32[16,2,128]{2,1,0:T(2,128)S(1)} %get-tuple-element.44, ...), kind=kOutput, calls=%fused_computation.45 | convolution fusion | flops 9437184 | bytes 2228224 | tf_op jit(solution)/shard_map/bhk,bhkv->bhv/dot_general | solution.py:62
  47.2 6.1 %fusion.5 = f32[16,2,1,128]{3,2,1,0:T(1,128)S(1)} fusion(f32[16,2,128,1]{2,3,1,0:T(1,128)S(1)} %bitcast.157, f32[16,2,128]{2,1,0:T(2,128)S(1)} %get-tuple-element.26, f32[16,2,128]{2,1,0:T(2,128)S(1)} %get-tuple-element.22, f32[16,2,128]{2,1,0:T(2,128)S(1)} %get-tuple-element.45, f32[16,2,128,128]{3,2,1,0:T(8,128)S(1)} %add_select_fusion, ...), kind=kOutput, calls=%fused_computation.9 | convolution fusion | flops 11010048 | bytes 2277376 | tf_op jit(solution)/shard_map/bhk,bhkv->bhv/dot_general | solution.py:62
  53.3 0.0 copy-start.6
  53.3 7.2 %fusion = f32[16,2,1,128]{3,2,1,0:T(1,128)S(1)} fusion(f32[16,2,128,1]{2,3,1,0:T(1,128)S(1)} %bitcast.156, f32[16,2,128]{2,1,0:T(2,128)S(1)} %get-tuple-element.25, f32[16,2,128]{2,1,0:T(2,128)S(1)} %get-tuple-element.21, f32[16,2,128]{2,1,0:T(2,128)S(1)} %get-tuple-element.46, f32[16,2,128]{2,1,0:T(2,128)S(1)} %get-tuple-element.26, ...), kind=kOutput, calls=%fused_computation | convolution fusion | flops 12582912 | bytes 2326528 | tf_op jit(solution)/shard_map/bhk,bhkv->bhv/dot_general | solution.py:62
  60.6 0.1 fusion.39
  60.8 0.1 mul.343
  60.9 0.1 mul.344
  61.0 0.0 copy-done
  61.0 2.8 %fusion.16 = f32[16,4,2048]{2,0,1:T(8,128)} fusion(bf16[1024,2048]{1,0:T(8,128)(2,1)} %param.19, s32[]{:T(128)S(6)} %select_n.20, f32[16,4,256]{2,0,1:T(8,128)S(1)} %mul.344, f32[16,1,256]{2,0,1:T(8,128)S(1)} %stack.28, f32[16,1,256]{2,0,1:T(8,128)S(1)} %stack.27, f32[16,1,256]{2,0,1:T(8,128)S(1)} %stack.26, f32[16,1,256]{2,0,1:T(8,128)S(1)} %stack.25, ...), kind=kOutput, calls=%fused_computation.24 | convolution fusion | flops 134430720 | bytes 3015684 | tf_op jit(solution)/shard_map/dot_general | solution.py:72
  63.8 0.0 all-gather.3.cloned.1.call-update
  63.9 24.1 %all-gather.3.cloned.1.call-done = f32[64,4,2048]{2,0,1:T(8,128)} async-done(((f32[16,4,2048]{2,0,1:T(8,128)}), f32[64,4,2048]{2,0,1:T(8,128)}) %all-gather.3.cloned.1.call-update) | async-done | bytes 2097168 | tf_op jit(solution)/shard_map/all_gather | solution.py:73
  88.0 1.8 %reduce_sum.38 = bf16[16,4,2048]{2,0,1:T(8,128)(2,1)S(1)} reduce(f32[4,16,4,2048]{3,1,0,2:T(8,128)} %bitcast.143, f32[]{:T(128)} %constant.13.clone.1), dimensions={0}, to_apply=%region_3.4 | reduce | flops 393216 | bytes 2359300 | tf_op jit(solution)/shard_map/reduce_sum | solution.py:73
  89.8 1.4 %copy.71 = bf16[16,4,2048]{0,1,2:T(4,128)(2,1)S(1)} copy(bf16[16,4,2048]{2,0,1:T(8,128)(2,1)S(1)} %reduce_sum.38) | data formatting | bytes 524288 | tf_op jit(solution)/shard_map/convert_element_type | solution.py:73
  91.1 2.2 %reshape.149 = bf16[8,2,8192]{2,1,0:T(2,128)(2,1)S(1)} reshape(bf16[2048,4,16]{2,1,0:T(4,128)(2,1)S(1)} %bitcast.141) | data formatting | bytes 524288
  93.3 14.7 %all_to_all.27 = bf16[8,2,8192]{2,1,0:T(2,128)(2,1)} all-to-all(bf16[8,2,8192]{2,1,0:T(2,128)(2,1)S(1)} %reshape.149), channel_id=1, replica_groups=mesh['kv'=8,'tp'=4] {'kv'}, dimensions={0} | all-to-all | bytes 524288 | tf_op jit(solution)/shard_map/all_to_all | solution.py:74
  108.0 2.4 %reshape.150 = bf16[2048,4,16]{2,1,0:T(4,128)(2,1)S(1)} reshape(bf16[8,2,8192]{2,1,0:T(2,128)(2,1)} %all_to_all.27) | data formatting | bytes 524288
  110.4 1.1 copy.84
  111.6 0.9 copy.74
  (18 shorter events, 0.3 us)
Async XLA Ops:
  7.2 53.8 %copy-start = (bf16[2048,256]{1,0:T(8,128)(2,1)S(1)}, bf16[2048,256]{1,0:T(8,128)(2,1)}, u32[]{:S(2)}) copy-start(bf16[2048,256]{1,0:T(8,128)(2,1)} %param.18) | copy-start | bytes 3145732
  7.2 20.7 %all-to-all-start = ((bf16[128,4,256]{2,1,0:T(4,128)(2,1)}), bf16[128,4,256]{2,1,0:T(4,128)(2,1)S(1)}, u32[]{:S(2)}, u32[]{:S(2)}) async-start(bf16[128,4,256]{2,1,0:T(4,128)(2,1)} %param.13), calls=%async_computation | async-start | bytes 524288 | tf_op jit(solution)/shard_map/all_to_all | solution.py:26
  14.6 73.4 %all-gather.3.cloned.1.call-start = ((), (), s32[]{:S(2)}) async-start(), calls=%async_computation.2 | async-start | bytes 2621440 | tf_op jit(solution)/shard_map/all_gather | solution.py:73
  15.3 0.6 copy-start.3
  27.8 25.5 %copy-start.1 = (f32[16,2,128,128]{3,2,1,0:T(8,128)}, f32[16,2,128,128]{3,2,1,0:T(8,128)S(1)}, u32[]{:S(2)}) copy-start(f32[16,2,128,128]{3,2,1,0:T(8,128)S(1)} %add_select_fusion) | copy-start | bytes 6291460
  27.8 3.5 %copy-start.5 = (f32[2048]{0:T(1024)S(1)}, f32[2048]{0:T(1024)}, u32[]{:S(2)}) copy-start(f32[2048]{0:T(1024)} %param.14) | copy-start | bytes 24580
  27.9 4.6 %copy-start.2 = (f32[256]{0:T(256)S(1)}, f32[256]{0:T(256)}, u32[]{:S(2)}) copy-start(f32[256]{0:T(256)} %param.20) | copy-start | bytes 3076
  27.9 4.6 %copy-start.4 = (f32[256]{0:T(256)S(1)}, f32[256]{0:T(256)}, u32[]{:S(2)}) copy-start(f32[256]{0:T(256)} %copy-done.3) | copy-start | bytes 3076
  53.3 7.7 %copy-start.6 = (f32[256]{0:T(256)S(1)}, f32[256]{0:T(256)}, u32[]{:S(2)}) copy-start(f32[256]{0:T(256)} %broadcast_bitcast_fusion) | copy-start | bytes 3076
Sparse Core Ops, SparseCore 0:
  64.0 23.9 all-gather.2
